TPU v7x, 32 devices: a whole 2x2x4 slice. The times are simulated.
32 devices in a mesh: sp: 8 (over z, x), tp: 4 (over y, core).
Axes of the slice: x: 2, y: 2, z: 4, core: 2. Of those that a mesh axis runs over, the one named last changes fastest.
Arguments:
- resid: bfloat16 [1024, 2048], P('sp'), may hold values from -8 to 8
- a_val: bfloat16 [1024, 1024], P('sp', 'tp'), may hold values from -8 to 8
- a_gate: bfloat16 [1024, 1024], P('sp', 'tp'), may hold values from -6 to 6
- conv_kernel: bfloat16 [31, 1024], P(None, 'tp'), may hold values from -1 to 1
- conv_bias: float32 [1024], P('tp'), may hold values from -3 to 3
- ln_gain: float32 [1024], P('tp'), may hold values from 0.1 to 1.9
- ln_bias: float32 [1024], P('tp'), may hold values from -3 to 3
- w_out: bfloat16 [1024, 2048], P('tp'), may hold values from -0.1875 to 0.1875
- ffn_gain: float32 [2048], replicated, may hold values from 0.1 to 1.9
- routes: int32 [1024, 4], P('sp'), may hold values from 0 to 7, all different within a row; in each aligned block of 128 rows (0 to 127, 128 to 255, ...) at most 128 rows name the same one
- route_weights: float32 [1024, 4], P('sp'), may hold values from 0.15 to 1.2
- exp_gate: bfloat16 [8, 2048, 4096], P('sp', None, 'tp'), may hold values from -0.125 to 0.125
- exp_up: bfloat16 [8, 2048, 4096], P('sp', None, 'tp'), may hold values from -0.125 to 0.125
- exp_down: bfloat16 [8, 4096, 2048], P('sp', None, 'tp'), may hold values from -0.09375 to 0.09375
- sh_gate: bfloat16 [2048, 512], P(None, 'tp'), may hold values from -0.125 to 0.125
- sh_up: bfloat16 [2048, 512], P(None, 'tp'), may hold values from -0.125 to 0.125
- sh_down: bfloat16 [512, 2048], P(None, 'tp'), may hold values from -0.25 to 0.25
Outputs:
- result: bfloat16 [1024, 2048], P('sp', 'tp')
Inputs may be any that keep to these rules, and one draw needn't show every extreme that they name: `routes`: among the 128 rows of one index of sp, each expert is named at most 128 times, a bound that some block reaches; a row names 4 different experts.
All inputs are finite; a program needn't handle non-finite values.
Results may differ from a plain program's by a relative error of at most 0.007.
Values may be sent and summed in bfloat16 or wider, within the bound.
A program may use at most 64 MiB of HBM per device.

v0:
```python
import jax
import jax.numpy as jnp
from jax import lax
from jax.sharding import PartitionSpec as P

LN_EPS = 1e-05
RMS_EPS = 1e-06


def shifted(value, axis, by):
    size = lax.axis_size(axis)
    pairs = [(i, i + by) for i in range(size) if 0 <= i + by < size]
    return lax.ppermute(value, axis, pairs)


def body(
    resid,
    a_val,
    a_gate,
    conv_kernel,
    conv_bias,
    ln_gain,
    ln_bias,
    w_out,
    ffn_gain,
    routes,
    route_weights,
    exp_gate,
    exp_up,
    exp_down,
    sh_gate,
    sh_up,
    sh_down,
):
    tp_count = lax.axis_size("tp")
    tp_place = lax.axis_index("tp")
    sp_count = lax.axis_size("sp")
    tok_rows = resid.shape[0]
    model_width = resid.shape[1]
    col_width = model_width // tp_count
    col_start = tp_place * col_width
    conv_span = conv_kernel.shape[0]
    channels_all = a_val.shape[1] * tp_count
    gated_in = (a_val.astype(jnp.float32) * jax.nn.sigmoid(a_gate.astype(jnp.float32))).astype(
        jnp.bfloat16
    )
    before = shifted(gated_in[tok_rows - (conv_span - 1) :], "sp", 1)
    padded = jnp.concatenate([before, gated_in], axis=0).astype(jnp.float32)
    kernel = conv_kernel.astype(jnp.float32)

    def add_tap(offset, running):
        window_rows = lax.dynamic_slice_in_dim(padded, offset, tok_rows, 0)
        return running + lax.dynamic_slice_in_dim(kernel, offset, 1, 0) * window_rows

    start_sum = jnp.broadcast_to(conv_bias[None, :], gated_in.shape)
    conv_out = lax.fori_loop(0, conv_span, add_tap, start_sum)
    row_sums = lax.psum((jnp.sum(conv_out, axis=1), jnp.sum(conv_out * conv_out, axis=1)), "tp")
    channel_mean = row_sums[0] / channels_all
    channel_var = row_sums[1] / channels_all - channel_mean * channel_mean
    scaled = (conv_out - channel_mean[:, None]) * lax.rsqrt(
        channel_var[:, None] + LN_EPS
    ) * ln_gain[None, :] + ln_bias[None, :]
    mixed_out = jax.nn.silu(scaled).astype(jnp.bfloat16)
    partial_proj = jnp.dot(mixed_out, w_out, preferred_element_type=jnp.float32)
    projected = lax.psum(partial_proj, "tp")
    middle = (resid.astype(jnp.float32) + projected).astype(jnp.bfloat16)
    middle_f = middle.astype(jnp.float32)
    inverse = lax.rsqrt(jnp.mean(middle_f * middle_f, axis=1, keepdims=True) + RMS_EPS)
    normed = (middle_f * inverse * ffn_gain[None, :]).astype(jnp.bfloat16)
    middle_cols = lax.dynamic_slice_in_dim(middle, col_start, col_width, 1)
    shared_gate = jnp.dot(normed, sh_gate, preferred_element_type=jnp.float32)
    shared_up = jnp.dot(normed, sh_up, preferred_element_type=jnp.float32)
    shared_hidden = (jax.nn.silu(shared_gate) * shared_up).astype(jnp.bfloat16)
    weight_rows = sh_down
    shared = jnp.dot(
        lax.all_gather(shared_hidden, "tp", axis=1, tiled=True),
        weight_rows,
        preferred_element_type=jnp.float32,
    )
    top_count = routes.shape[1]
    local_experts = exp_gate.shape[0]
    experts_all = local_experts * sp_count
    capacity = max(2 * tok_rows * top_count // experts_all, tp_count)
    pair_count = tok_rows * top_count
    chosen = routes.reshape(pair_count)
    one_hot = (chosen[:, None] == jnp.arange(experts_all, dtype=jnp.int32)[None, :]).astype(
        jnp.int32
    )
    earlier = jnp.cumsum(one_hot, axis=0) - one_hot
    place_in = jnp.sum(earlier * one_hot, axis=1)
    slot_of = chosen * capacity + place_in
    owner_ids = (
        jnp.zeros((experts_all * capacity,), jnp.int32)
        .at[slot_of]
        .set(jnp.arange(pair_count, dtype=jnp.int32) + 1)
    )
    owner_grid = owner_ids.reshape(sp_count, local_experts, capacity)
    part_slots = capacity // tp_count
    own_owners = lax.dynamic_slice_in_dim(owner_grid, tp_place * part_slots, part_slots, 2)
    source_row = jnp.maximum(own_owners - 1, 0) // top_count
    taken = normed[source_row.reshape(-1)].reshape(own_owners.shape + (model_width,))
    landed = lax.all_to_all(
        jnp.where((own_owners > 0)[..., None], taken, jnp.zeros((), jnp.bfloat16)),
        "sp",
        split_axis=0,
        concat_axis=0,
        tiled=True,
    )
    arrived = lax.all_gather(landed, "tp", axis=2, tiled=True)
    gate_part = jnp.einsum("sxcd,xdf->sxcf", arrived, exp_gate, preferred_element_type=jnp.float32)
    up_part = jnp.einsum("sxcd,xdf->sxcf", arrived, exp_up, preferred_element_type=jnp.float32)
    expert_hidden = (jax.nn.silu(gate_part) * up_part).astype(jnp.bfloat16)
    weight_rows = exp_down
    expert_sum = jnp.einsum(
        "sxcf,xfd->sxcd",
        lax.all_gather(expert_hidden, "tp", axis=3, tiled=True),
        weight_rows,
        preferred_element_type=jnp.float32,
    )
    expert_out = expert_sum.astype(jnp.bfloat16)
    returned = lax.all_to_all(expert_out, "sp", split_axis=0, concat_axis=0, tiled=True)
    flat_out = returned.reshape(experts_all * capacity, col_width)
    picked = flat_out[slot_of].astype(jnp.float32).reshape(tok_rows, top_count, col_width)
    routed = jnp.sum(picked * route_weights[:, :, None], axis=1)
    return (middle_cols.astype(jnp.float32) + shared + routed).astype(jnp.bfloat16)


def solution(mesh):
    in_specs = (
        P("sp", None),
        P("sp", "tp"),
        P("sp", "tp"),
        P(None, "tp"),
        P("tp"),
        P("tp"),
        P("tp"),
        P("tp", None),
        P(),
        P("sp", None),
        P("sp", None),
        P("sp", None, "tp"),
        P("sp", None, "tp"),
        P("sp", None, "tp"),
        P(None, "tp"),
        P(None, "tp"),
        P(None, "tp"),
    )
    out_specs = P("sp", "tp")
    return jax.shard_map(body, mesh=mesh, in_specs=in_specs, out_specs=out_specs, check_vma=False)
```

profile of v0, /device:TPU:0, one launch (start us, length us, event | category | flops | bytes accessed | tf_op | source)
XLA Modules:
  0.0 262.0 jit_solution(12313480295030517520)
XLA Ops:
  6.5 1.0 multiply_convert_fusion.1
  7.6 4.9 %collective-permute-start = (bf16[30,256]{1,0:T(8,128)(2,1)S(1)}, bf16[30,256]{1,0:T(8,128)(2,1)S(1)}, u32[]{:S(2)}, u32[]{:S(2)}) collective-permute-start(bf16[30,256]{1,0:T(8,128)(2,1)S(1)} %slice.16), channel_id=1, source_target_pairs={{0,4},{4,8},{8,12},{12,16},{16,20},{20,24},{24,28},{1,5},{5,9},{9,... | collective-permute-start | bytes 46088 | tf_op jit(solution)/shard_map/ppermute | solution.py:13
  14.4 1.1 reduce-window.6
  16.7 2.4 scatter_custom_fusion
  19.8 2.4 while.13
  22.4 6.3 %all-reduce = (f32[128]{0:T(128)S(1)}, f32[128]{0:T(128)S(1)}) all-reduce(f32[128]{0:T(128)S(1)} %get-tuple-element.86, f32[128]{0:T(128)S(1)} %get-tuple-element.85), channel_id=1, replica_groups=mesh['sp'=8,'tp'=4] {'tp'}, use_global_device_ids=true, to_apply=%region_5.0 | all-reduce | flops 256 | bytes 2048 | tf_op jit(solution)/shard_map/psum | solution.py:57
  28.7 2.1 fusion.33
  31.2 36.0 %all-reduce.3.cloned.1.call-done = f32[128,2048]{1,0:T(8,128)} async-done(((f32[128,2048]{1,0:T(8,128)}), f32[128,2048]{1,0:T(8,128)}) %all-reduce.3.cloned.1.call-update) | async-done | bytes 1048592 | tf_op jit(solution)/shard_map/psum | solution.py:65
  67.2 1.5 fusion.30
  68.9 1.4 gather_fusion
  70.4 30.6 %all_to_all.10 = bf16[8,1,32,2048]{3,2,1,0:T(8,128)(2,1)} all-to-all(bf16[8,1,32,2048]{3,2,1,0:T(8,128)(2,1)S(1)} %broadcast_select_fusion), channel_id=1, replica_groups=mesh['sp'=8,'tp'=4] {'sp'}, dimensions={0} | all-to-all | bytes 2097152 | tf_op jit(solution)/shard_map/all_to_all | solution.py:102
  101.1 33.4 %all-gather.3.cloned.1.call-done = bf16[8,1,128,2048]{3,2,0,1:T(8,128)(2,1)} async-done(((bf16[8,1,32,2048]{3,2,0,1:T(8,128)(2,1)}), bf16[8,1,128,2048]{3,2,0,1:T(8,128)(2,1)}) %all-gather.3.cloned.1.call-update) | async-done | bytes 4194320 | tf_op jit(solution)/shard_map/all_gather | solution.py:109
  134.6 7.7 %fusion.4 = f32[8,128,1024]{2,1,0:T(8,128)S(1)} fusion(bf16[1,2048,1024]{2,1,0:T(8,128)(2,1)} %param.31, bf16[8,1,128,2048]{3,2,0,1:T(8,128)(2,1)} %all-gather.3.cloned.1.call-done), kind=kOutput, calls=%fused_computation.10 | convolution fusion | flops 4294967296 | bytes 12582912 | tf_op jit(solution)/shard_map/sxcd,xdf->sxcf/dot_general | solution.py:111
  142.2 6.4 %fusion.2 = bf16[8,1,128,1024]{3,2,0,1:T(8,128)(2,1)} fusion(f32[8,128,1024]{2,1,0:T(8,128)S(1)} %fusion.4, bf16[1,2048,1024]{2,1,0:T(8,128)(2,1)S(1)} %copy-done.4, bf16[8,1,128,2048]{3,2,0,1:T(8,128)(2,1)S(1)} %copy-done.5), kind=kOutput, calls=%fused_computation.8 | convolution fusion | flops 4301258752 | bytes 14680064 | tf_op jit(solution)/shard_map/sxcd,xdf->sxcf/dot_general | solution.py:110
  148.6 58.4 %all-gather.5.cloned.1.call-done = bf16[8,1,128,4096]{3,2,0,1:T(8,128)(2,1)} async-done(((bf16[8,1,128,1024]{3,2,0,1:T(8,128)(2,1)}), bf16[8,1,128,4096]{3,2,0,1:T(8,128)(2,1)}) %all-gather.5.cloned.1.call-update) | async-done | bytes 8388624 | tf_op jit(solution)/shard_map/all_gather | solution.py:116
  207.0 10.1 %fusion.22 = bf16[8,1,128,512]{3,2,1,0:T(8,128)(2,1)} fusion(bf16[1,4096,512]{2,1,0:T(8,128)(2,1)} %param.32, bf16[8,1,128,4096]{3,2,0,1:T(8,128)(2,1)} %all-gather.5.cloned.1.call-done), kind=kOutput, calls=%fused_computation.22 | convolution fusion | flops 4295491584 | bytes 13631488 | tf_op jit(solution)/shard_map/sxcf,xfd->sxcd/dot_general | solution.py:114
  217.2 5.5 %all-to-all-start.1 = ((bf16[8,1,128,512]{3,2,1,0:T(8,128)(2,1)}), bf16[8,1,128,512]{3,2,1,0:T(8,128)(2,1)S(1)}, u32[]{:S(2)}, u32[]{:S(2)}) async-start(bf16[8,1,128,512]{3,2,1,0:T(8,128)(2,1)} %fusion.22), calls=%async_computation.1 | async-start | bytes 2097152 | tf_op jit(solution)/shard_map/all_to_all | solution.py:121
  222.8 1.3 fusion.47
  224.1 1.3 fusion.29
  225.5 5.4 %all_gather.9 = bf16[128,512]{1,0:T(8,128)(2,1)S(1)} all-gather(bf16[128,128]{1,0:T(8,128)(2,1)S(1)} %fusion.29), channel_id=1, replica_groups=mesh['sp'=8,'tp'=4] {'tp'}, dimensions={1}, use_global_device_ids=true | all-gather | bytes 163840 | tf_op jit(solution)/shard_map/all_gather | solution.py:76
  230.9 17.9 %all-to-all-done.1 = bf16[8,1,128,512]{3,2,1,0:T(8,128)(2,1)S(1)} async-done(((bf16[8,1,128,512]{3,2,1,0:T(8,128)(2,1)}), bf16[8,1,128,512]{3,2,1,0:T(8,128)(2,1)S(1)}, u32[]{:S(2)}, u32[]{:S(2)}) %all-to-all-start.1) | async-done | bytes 1048608 | tf_op jit(solution)/shard_map/all_to_all | solution.py:121
  248.9 2.6 gather_fusion.1
  251.5 1.4 reshape.152
  253.6 1.9 fusion.28
  (111 shorter events, 6.9 us)
Async XLA Ops:
  6.5 22.2 %copy-start = (bf16[256,2048]{1,0:T(8,128)(2,1)S(1)}, bf16[256,2048]{1,0:T(8,128)(2,1)}, u32[]{:S(2)}) copy-start(bf16[256,2048]{1,0:T(8,128)(2,1)} %param.26) | copy-start | bytes 3145732
  6.5 60.7 %copy-start.1 = (bf16[128,2048]{1,0:T(8,128)(2,1)S(1)}, bf16[128,2048]{1,0:T(8,128)(2,1)}, u32[]{:S(2)}) copy-start(bf16[128,2048]{1,0:T(8,128)(2,1)} %param.19) | copy-start | bytes 1572868
  6.5 60.6 %all-reduce.3.cloned.1.call-start = ((), (), s32[]{:S(2)}) async-start(), calls=%async_computation.2 | async-start | bytes 2097152 | tf_op jit(solution)/shard_map/psum | solution.py:65
  7.6 11.5 %collective-permute-start = (bf16[30,256]{1,0:T(8,128)(2,1)S(1)}, bf16[30,256]{1,0:T(8,128)(2,1)S(1)}, u32[]{:S(2)}, u32[]{:S(2)}) collective-permute-start(bf16[30,256]{1,0:T(8,128)(2,1)S(1)} %slice.16), channel_id=1, source_target_pairs={{0,4},{4,8},{8,12},{12,16},{16,20},{20,24},{24,28},{1,5},{5,9},{9,... | collective-permute-start | bytes 46088 | tf_op jit(solution)/shard_map/ppermute | solution.py:13
  14.2 54.5 %copy-start.2 = (f32[2048]{0:T(1024)S(1)}, f32[2048]{0:T(1024)}, u32[]{:S(2)}) copy-start(f32[2048]{0:T(1024)} %param.27) | copy-start | bytes 24580
  30.9 103.7 %all-gather.3.cloned.1.call-start = ((), (), s32[]{:S(2)}) async-start(), calls=%async_computation.3 | async-start | bytes 5242880 | tf_op jit(solution)/shard_map/all_gather | solution.py:109
  101.1 106.0 %all-gather.5.cloned.1.call-start = ((), (), s32[]{:S(2)}) async-start(), calls=%async_computation.4 | async-start | bytes 10485760 | tf_op jit(solution)/shard_map/all_gather | solution.py:116
  134.5 7.7 %copy-start.4 = (bf16[1,2048,1024]{2,1,0:T(8,128)(2,1)S(1)}, bf16[1,2048,1024]{2,1,0:T(8,128)(2,1)}, u32[]{:S(2)}) copy-start(bf16[1,2048,1024]{2,1,0:T(8,128)(2,1)} %param.30) | copy-start | bytes 12582916
  134.5 7.7 %copy-start.5 = (bf16[8,1,128,2048]{3,2,0,1:T(8,128)(2,1)S(1)}, bf16[8,1,128,2048]{3,2,0,1:T(8,128)(2,1)}, u32[]{:S(2)}) copy-start(bf16[8,1,128,2048]{3,2,0,1:T(8,128)(2,1)} %all-gather.3.cloned.1.call-done) | copy-start | bytes 12582916
  148.6 74.0 %copy-start.3 = (f32[128,4]{0,1:T(4,128)S(1)}, f32[128,4]{0,1:T(4,128)}, u32[]{:S(2)}) copy-start(f32[128,4]{0,1:T(4,128)} %param.29) | copy-start | bytes 6148
  217.2 31.7 %all-to-all-start.1 = ((bf16[8,1,128,512]{3,2,1,0:T(8,128)(2,1)}), bf16[8,1,128,512]{3,2,1,0:T(8,128)(2,1)S(1)}, u32[]{:S(2)}, u32[]{:S(2)}) async-start(bf16[8,1,128,512]{3,2,1,0:T(8,128)(2,1)} %fusion.22), calls=%async_computation.1 | async-start | bytes 2097152 | tf_op jit(solution)/shard_map/all_to_all | solution.py:121
Sparse Core Ops, SparseCore 0:
  31.0 36.1 all-reduce.2
  101.2 33.3 all-gather.2
  148.7 58.2 all-gather.4
where the time goes:
time: 263 us; the launch traced here: 262 us
  waiting for transfers between devices  146 us (56%)
  blocking collectives  42.4 us (16%)
  matrix products  30.9 us (12%)
  between operations  13.3 us (5%)
  starting transfers between devices  10.5 us (4%)
  local copies, waits for them, and re-layouts  10.4 us (4%)
  other arithmetic  7.78 us (3%)
    all_gather x1, waiting for transfers between devices, body(): lax.all_gather(expert_hidden, 'tp', axis=3, tiled=True)  58.4 us
    psum x1, waiting for transfers between devices, body(): projected = lax.psum(partial_proj, 'tp')  36 us
    all_gather x1, waiting for transfers between devices, body(): arrived = lax.all_gather(landed, 'tp', axis=2, tiled=True)  33.4 us
    all_to_all x1, blocking collectives, body(): lax.all_to_all(jnp.where((own_owners > 0)[..., None], taken, jnp.zeros(()...  30.6 us
    all_to_all x1, waiting for transfers between devices, body(): lax.all_to_all(expert_out, 'sp', split_axis=0, concat_axis=0, tiled=True)  17.9 us
    dot_general x1, matrix products, body(): jnp.einsum('sxcf,xfd->sxcd', lax.all_gather(expert_hidden, 'tp', axis=3,...  10.1 us
    dot_general x1, matrix products, body(): jnp.einsum('sxcd,xdf->sxcf', arrived, exp_up, preferred_element_type=jnp....  7.65 us
    dot_general x1, matrix products, body(): jnp.einsum('sxcd,xdf->sxcf', arrived, exp_gate, preferred_element_type=jn...  6.37 us
  transfers between devices with their start and end apart: 5, of which 4 were waited for; matrix products, arithmetic and copies ran while one was open for 4% of the time, Pallas kernels for 0%

commit v1 on v0

--- a/solution.py
+++ b/solution.py
@@ -111,12 +111,22 @@
     up_part = jnp.einsum("sxcd,xdf->sxcf", arrived, exp_up, preferred_element_type=jnp.float32)
     expert_hidden = (jax.nn.silu(gate_part) * up_part).astype(jnp.bfloat16)
     weight_rows = exp_down
-    expert_sum = jnp.einsum(
-        "sxcf,xfd->sxcd",
-        lax.all_gather(expert_hidden, "tp", axis=3, tiled=True),
-        weight_rows,
-        preferred_element_type=jnp.float32,
-    )
+    length, index, rows = (lax.axis_size("tp"), lax.axis_index("tp"), expert_hidden.shape[3])
+    right = [(i_2, (i_2 + 1) % length) for i_2 in range(length)]
+    current, total = (expert_hidden, None)
+    for lap in range(length):
+        coming = lax.ppermute(current, "tp", right) if lap < length - 1 else None
+        take_in = jnp.einsum(
+            "sxcf,xfd->sxcd",
+            current,
+            lax.dynamic_slice_in_dim(
+                weight_rows, (index - lap) % length * rows, current.shape[3], axis=1
+            ),
+            preferred_element_type=jnp.float32,
+        )
+        total = take_in if total is None else total + take_in
+        current = coming
+    expert_sum = total
     expert_out = expert_sum.astype(jnp.bfloat16)
     returned = lax.all_to_all(expert_out, "sp", split_axis=0, concat_axis=0, tiled=True)
     flat_out = returned.reshape(experts_all * capacity, col_width)

time: 263 us -> 275 us (1.046)
  waiting for transfers between devices: 146 us -> 155 us
  local copies, waits for them, and re-layouts: 10.4 us -> 13.2 us
    ppermute x0 -> x3, waiting for transfers between devices: none -> 68.5 us  [body(): coming = lax.ppermute(current, 'tp', right) if lap < length - 1 else None]
    all_gather x1 -> x0, waiting for transfers between devices: 58.4 us -> none  [body(): lax.all_gather(expert_hidden, 'tp', axis=3, tiled=True)]
    unnamed x14 -> x28, local copies, waits for them, and re-layouts: 0.93 us -> 4.88 us
    dot_general x1 -> x4, matrix products: 10.1 us -> 11.5 us  [body(): jnp.einsum('sxcf,xfd->sxcd', current, lax.dynamic_slice_in_dim(weight_row...]
  transfers between devices with their start and end apart: 5 -> 7, of which waited for: 4 -> 6; matrix products, arithmetic and copies ran while one was open for 4% -> 6% of each run, Pallas kernels for 0% -> 0%
where the time goes in v1:
time: 275 us; the launch traced here: 274 us
  waiting for transfers between devices  155 us (56%)
  blocking collectives  42.4 us (15%)
  matrix products  30.1 us (11%)
  between operations  13.7 us (5%)
  local copies, waits for them, and re-layouts  13.2 us (5%)
  starting transfers between devices  10.7 us (4%)
  other arithmetic  7.79 us (3%)
    ppermute x3, waiting for transfers between devices, body(): coming = lax.ppermute(current, 'tp', right) if lap < length - 1 else None  68.5 us
    psum x1, waiting for transfers between devices, body(): projected = lax.psum(partial_proj, 'tp')  36 us
    all_gather x1, waiting for transfers between devices, body(): arrived = lax.all_gather(landed, 'tp', axis=2, tiled=True)  33.5 us
    all_to_all x1, blocking collectives, body(): lax.all_to_all(jnp.where((own_owners > 0)[..., None], taken, jnp.zeros(()...  30.6 us
    all_to_all x1, waiting for transfers between devices, body(): lax.all_to_all(expert_out, 'sp', split_axis=0, concat_axis=0, tiled=True)  17.1 us
    dot_general x4, matrix products, body(): jnp.einsum('sxcf,xfd->sxcd', current, lax.dynamic_slice_in_dim(weight_row...  11.5 us
    dot_general x1, matrix products, body(): jnp.einsum('sxcd,xdf->sxcf', arrived, exp_up, preferred_element_type=jnp....  7.64 us
    psum x1, blocking collectives, body(): lax.psum((jnp.sum(conv_out, axis=1), jnp.sum(conv_out * conv_out, axis=1)...  6.33 us
  transfers between devices with their start and end apart: 7, of which 6 were waited for; matrix products, arithmetic and copies ran while one was open for 6% of the time, Pallas kernels for 0%

profile of v1, /device:TPU:0, one launch (start us, length us, event | category | flops | bytes accessed | tf_op | source)
XLA Modules:
  0.0 273.9 jit_solution(17125835515036135828)
XLA Ops:
  7.6 4.9 %collective-permute-start = (bf16[30,256]{1,0:T(8,128)(2,1)S(1)}, bf16[30,256]{1,0:T(8,128)(2,1)S(1)}, u32[]{:S(2)}, u32[]{:S(2)}) collective-permute-start(bf16[30,256]{1,0:T(8,128)(2,1)S(1)} %slice.16), channel_id=1, source_target_pairs={{0,4},{4,8},{8,12},{12,16},{16,20},{20,24},{24,28},{1,5},{5,9},{9,... | collective-permute-start | bytes 46088 | tf_op jit(solution)/shard_map/ppermute | solution.py:13
  16.7 2.4 scatter_custom_fusion
  19.8 2.4 while.13
  22.4 6.3 %all-reduce = (f32[128]{0:T(128)S(1)}, f32[128]{0:T(128)S(1)}) all-reduce(f32[128]{0:T(128)S(1)} %get-tuple-element.86, f32[128]{0:T(128)S(1)} %get-tuple-element.85), channel_id=1, replica_groups=mesh['sp'=8,'tp'=4] {'tp'}, use_global_device_ids=true, to_apply=%region_5.0 | all-reduce | flops 256 | bytes 2048 | tf_op jit(solution)/shard_map/psum | solution.py:57
  28.7 2.1 fusion.41
  31.2 36.0 %all-reduce.3.cloned.1.call-done = f32[128,2048]{1,0:T(8,128)} async-done(((f32[128,2048]{1,0:T(8,128)}), f32[128,2048]{1,0:T(8,128)}) %all-reduce.3.cloned.1.call-update) | async-done | bytes 1048592 | tf_op jit(solution)/shard_map/psum | solution.py:65
  67.2 1.5 fusion.30
  69.7 1.4 gather_fusion
  71.2 30.6 %all_to_all.10 = bf16[8,1,32,2048]{3,2,1,0:T(8,128)(2,1)} all-to-all(bf16[8,1,32,2048]{3,2,1,0:T(8,128)(2,1)S(1)} %broadcast_select_fusion), channel_id=1, replica_groups=mesh['sp'=8,'tp'=4] {'sp'}, dimensions={0} | all-to-all | bytes 2097152 | tf_op jit(solution)/shard_map/all_to_all | solution.py:102
  101.9 33.5 %all-gather.2.cloned.1.call-done = bf16[8,1,128,2048]{3,2,0,1:T(8,128)(2,1)} async-done(((bf16[8,1,32,2048]{3,2,0,1:T(8,128)(2,1)}), bf16[8,1,128,2048]{3,2,0,1:T(8,128)(2,1)}) %all-gather.2.cloned.1.call-update) | async-done | bytes 4194320 | tf_op jit(solution)/shard_map/all_gather | solution.py:109
  135.4 7.6 %fusion.1 = f32[8,128,1024]{2,1,0:T(8,128)S(1)} fusion(bf16[1,2048,1024]{2,1,0:T(8,128)(2,1)} %param.31, bf16[8,1,128,2048]{3,2,0,1:T(8,128)(2,1)} %all-gather.2.cloned.1.call-done), kind=kOutput, calls=%fused_computation.7 | convolution fusion | flops 4294967296 | bytes 12582912 | tf_op jit(solution)/shard_map/sxcd,xdf->sxcf/dot_general | solution.py:111
  143.1 5.4 %fusion = bf16[8,1,128,1024]{3,2,0,1:T(8,128)(2,1)S(1)} fusion(f32[8,128,1024]{2,1,0:T(8,128)S(1)} %fusion.1, bf16[1,2048,1024]{2,1,0:T(8,128)(2,1)S(1)} %copy-done.7, bf16[8,1,128,2048]{3,2,0,1:T(8,128)(2,1)S(1)} %copy-done.9), kind=kOutput, calls=%fused_computation.6 | convolution fusion | flops 4301258752 | bytes 14680064 | tf_op jit(solution)/shard_map/sxcd,xdf->sxcf/dot_general | solution.py:110
  150.0 25.2 %collective-permute-done.1 = bf16[8,1,128,1024]{3,2,0,1:T(8,128)(2,1)S(1)} collective-permute-done((bf16[8,1,128,1024]{3,2,0,1:T(8,128)(2,1)S(1)}, bf16[8,1,128,1024]{3,2,0,1:T(8,128)(2,1)S(1)}, u32[]{:S(2)}, u32[]{:S(2)}) %collective-permute-start.1) | collective-permute-done | bytes 2097184 | tf_op jit(solution)/shard_map/ppermute | solution.py:118
  175.2 1.3 copy-done.11
  176.6 25.6 %collective-permute-done.2 = bf16[8,1,128,1024]{3,2,0,1:T(8,128)(2,1)} collective-permute-done((bf16[8,1,128,1024]{3,2,0,1:T(8,128)(2,1)S(1)}, bf16[8,1,128,1024]{3,2,0,1:T(8,128)(2,1)}, u32[]{:S(2)}, u32[]{:S(2)}) %collective-permute-start.2) | collective-permute-done | bytes 2097184 | tf_op jit(solution)/shard_map/ppermute | solution.py:118
  202.1 3.4 %fusion.20 = f32[512,8,128]{2,0,1:T(8,128)S(1)} fusion(bf16[8,1,128,1024]{3,2,0,1:T(8,128)(2,1)} %copy-done.10, bf16[1,4096,512]{2,1,0:T(8,128)(2,1)} %param.32, s32[]{:T(128)S(6)} %select_n.87), kind=kOutput, calls=%fused_computation.24 | convolution fusion | flops 1073741824 | bytes 5242884 | tf_op jit(solution)/shard_map/sxcf,xfd->sxcd/dot_general | solution.py:119
  207.2 2.9 %fusion.16 = f32[512,8,128]{2,0,1:T(8,128)S(1)} fusion(bf16[8,1,128,1024]{3,2,0,1:T(8,128)(2,1)} %collective-permute-done.2, bf16[1,4096,512]{2,1,0:T(8,128)(2,1)S(1)} %copy-done.8, s32[]{:T(128)S(6)} %select_n.96), kind=kOutput, calls=%fused_computation.20 | convolution fusion | flops 1073741824 | bytes 5242884 | tf_op jit(solution)/shard_map/sxcf,xfd->sxcd/dot_general | solution.py:119
  210.2 17.7 %collective-permute-done.3 = bf16[8,1,128,1024]{3,2,0,1:T(8,128)(2,1)} collective-permute-done((bf16[8,1,128,1024]{3,2,0,1:T(8,128)(2,1)}, bf16[8,1,128,1024]{3,2,0,1:T(8,128)(2,1)}, u32[]{:S(2)}, u32[]{:S(2)}) %collective-permute-start.3) | collective-permute-done | bytes 2097184 | tf_op jit(solution)/shard_map/ppermute | solution.py:118
  227.9 4.0 %fusion.24 = bf16[8,1,128,512]{2,3,1,0:T(8,128)(2,1)} fusion(bf16[8,1,128,1024]{3,2,0,1:T(8,128)(2,1)} %collective-permute-done.3, f32[512,8,128]{2,0,1:T(8,128)S(1)} %fusion.16, f32[512,8,128]{2,0,1:T(8,128)S(1)} %fusion.20, f32[512,8,128]{2,0,1:T(8,128)S(1)} %fusion.18, bf16[1,4096,512]{2,1,0:T(8,128)(2,1)S(1)} %copy-done.8, s32[]{:T(128)S(6)} %select_n.98), kind=kOutput, calls=%fused_computation.27 | convolution fusion | flops 1075838976 | bytes 10485764 | tf_op jit(solution)/shard_map/sxcf,xfd->sxcd/dot_general | solution.py:119
  231.9 5.5 %all-to-all-start.1 = ((bf16[8,1,128,512]{2,3,1,0:T(8,128)(2,1)}), bf16[8,1,128,512]{2,3,1,0:T(8,128)(2,1)S(1)}, u32[]{:S(2)}, u32[]{:S(2)}) async-start(bf16[8,1,128,512]{2,3,1,0:T(8,128)(2,1)} %fusion.24), calls=%async_computation.1 | async-start | bytes 2097152 | tf_op jit(solution)/shard_map/all_to_all | solution.py:131
  239.2 5.4 %all_gather.6 = bf16[128,512]{1,0:T(8,128)(2,1)S(1)} all-gather(bf16[128,128]{1,0:T(8,128)(2,1)S(1)} %fusion.29), channel_id=1, replica_groups=mesh['sp'=8,'tp'=4] {'tp'}, dimensions={1}, use_global_device_ids=true | all-gather | bytes 163840 | tf_op jit(solution)/shard_map/all_gather | solution.py:76
  244.6 17.1 %all-to-all-done.1 = bf16[8,1,128,512]{2,3,1,0:T(8,128)(2,1)S(1)} async-done(((bf16[8,1,128,512]{2,3,1,0:T(8,128)(2,1)}), bf16[8,1,128,512]{2,3,1,0:T(8,128)(2,1)S(1)}, u32[]{:S(2)}, u32[]{:S(2)}) %all-to-all-start.1) | async-done | bytes 1048608 | tf_op jit(solution)/shard_map/all_to_all | solution.py:131
  262.3 2.0 gather_fusion.1
  265.3 1.8 fusion.28
  (132 shorter events, 15.7 us)
Async XLA Ops:
  6.5 22.2 %copy-start = (bf16[256,2048]{1,0:T(8,128)(2,1)S(1)}, bf16[256,2048]{1,0:T(8,128)(2,1)}, u32[]{:S(2)}) copy-start(bf16[256,2048]{1,0:T(8,128)(2,1)} %param.26) | copy-start | bytes 3145732
  6.5 60.7 %copy-start.2 = (bf16[128,2048]{1,0:T(8,128)(2,1)S(1)}, bf16[128,2048]{1,0:T(8,128)(2,1)}, u32[]{:S(2)}) copy-start(bf16[128,2048]{1,0:T(8,128)(2,1)} %param.19) | copy-start | bytes 1572868
  6.5 60.7 %all-reduce.3.cloned.1.call-start = ((), (), s32[]{:S(2)}) async-start(), calls=%async_computation.2 | async-start | bytes 2097152 | tf_op jit(solution)/shard_map/psum | solution.py:65
  7.6 11.5 %collective-permute-start = (bf16[30,256]{1,0:T(8,128)(2,1)S(1)}, bf16[30,256]{1,0:T(8,128)(2,1)S(1)}, u32[]{:S(2)}, u32[]{:S(2)}) collective-permute-start(bf16[30,256]{1,0:T(8,128)(2,1)S(1)} %slice.16), channel_id=1, source_target_pairs={{0,4},{4,8},{8,12},{12,16},{16,20},{20,24},{24,28},{1,5},{5,9},{9,... | collective-permute-start | bytes 46088 | tf_op jit(solution)/shard_map/ppermute | solution.py:13
  14.2 55.3 %copy-start.5 = (f32[2048]{0:T(1024)S(1)}, f32[2048]{0:T(1024)}, u32[]{:S(2)}) copy-start(f32[2048]{0:T(1024)} %param.27) | copy-start | bytes 24580
  30.9 104.5 %all-gather.2.cloned.1.call-start = ((), (), s32[]{:S(2)}) async-start(), calls=%async_computation.3 | async-start | bytes 5242880 | tf_op jit(solution)/shard_map/all_gather | solution.py:109
  68.7 0.8 copy-start.1
  135.4 7.7 %copy-start.7 = (bf16[1,2048,1024]{2,1,0:T(8,128)(2,1)S(1)}, bf16[1,2048,1024]{2,1,0:T(8,128)(2,1)}, u32[]{:S(2)}) copy-start(bf16[1,2048,1024]{2,1,0:T(8,128)(2,1)} %param.30) | copy-start | bytes 12582916
  135.4 7.7 %copy-start.9 = (bf16[8,1,128,2048]{3,2,0,1:T(8,128)(2,1)S(1)}, bf16[8,1,128,2048]{3,2,0,1:T(8,128)(2,1)}, u32[]{:S(2)}) copy-start(bf16[8,1,128,2048]{3,2,0,1:T(8,128)(2,1)} %all-gather.2.cloned.1.call-done) | copy-start | bytes 12582916
  148.4 1.3 copy-start.10
  149.7 25.5 %collective-permute-start.1 = (bf16[8,1,128,1024]{3,2,0,1:T(8,128)(2,1)S(1)}, bf16[8,1,128,1024]{3,2,0,1:T(8,128)(2,1)S(1)}, u32[]{:S(2)}, u32[]{:S(2)}) collective-permute-start(bf16[8,1,128,1024]{3,2,0,1:T(8,128)(2,1)S(1)} %fusion), channel_id=1, source_target_pairs={{0,1},{1,2},{2,3},{3,0},{4,5},{5,6},{6,7},{7,4},{8,9},{9,10},{10,1... | collective-permute-start | bytes 6291464 | tf_op jit(solution)/shard_map/ppermute | solution.py:118
  175.2 1.3 copy-start.11
  176.6 25.6 %collective-permute-start.2 = (bf16[8,1,128,1024]{3,2,0,1:T(8,128)(2,1)S(1)}, bf16[8,1,128,1024]{3,2,0,1:T(8,128)(2,1)}, u32[]{:S(2)}, u32[]{:S(2)}) collective-permute-start(bf16[8,1,128,1024]{3,2,0,1:T(8,128)(2,1)S(1)} %collective-permute-done.1), channel_id=1, source_target_pairs={{0,1},{1,2},{2,3},{3,0},{4,5},{5,6},{6,7},{7,4},{8,9},{9,10},{10,1... | collective-permute-start | bytes 6291464 | tf_op jit(solution)/shard_map/ppermute | solution.py:118
  202.1 25.8 %collective-permute-start.3 = (bf16[8,1,128,1024]{3,2,0,1:T(8,128)(2,1)}, bf16[8,1,128,1024]{3,2,0,1:T(8,128)(2,1)}, u32[]{:S(2)}, u32[]{:S(2)}) collective-permute-start(bf16[8,1,128,1024]{3,2,0,1:T(8,128)(2,1)} %collective-permute-done.2), channel_id=1, source_target_pairs={{0,1},{1,2},{2,3},{3,0},{4,5},{5,6},{6,7},{7,4},{8,9},{9,10},{10,1... | collective-permute-start | bytes 6291464 | tf_op jit(solution)/shard_map/ppermute | solution.py:118
  202.1 3.4 %copy-start.8 = (bf16[1,4096,512]{2,1,0:T(8,128)(2,1)S(1)}, bf16[1,4096,512]{2,1,0:T(8,128)(2,1)}, u32[]{:S(2)}) copy-start(bf16[1,4096,512]{2,1,0:T(8,128)(2,1)} %param.32) | copy-start | bytes 12582916
  202.1 3.8 %copy-start.12 = (bf16[8,1,128,1024]{3,2,0,1:T(8,128)(2,1)S(1)}, bf16[8,1,128,1024]{3,2,0,1:T(8,128)(2,1)}, u32[]{:S(2)}) copy-start(bf16[8,1,128,1024]{3,2,0,1:T(8,128)(2,1)} %copy-done.11) | copy-start | bytes 6291460
  210.1 27.3 %copy-start.6 = (f32[128,4]{0,1:T(4,128)S(1)}, f32[128,4]{0,1:T(4,128)}, u32[]{:S(2)}) copy-start(f32[128,4]{0,1:T(4,128)} %param.29) | copy-start | bytes 6148
  210.2 27.4 %copy-start.3 = (bf16[2048,128]{1,0:T(8,128)(2,1)S(1)}, bf16[2048,128]{1,0:T(8,128)(2,1)}, u32[]{:S(2)}) copy-start(bf16[2048,128]{1,0:T(8,128)(2,1)} %param.33) | copy-start | bytes 1572868
  231.9 29.9 %all-to-all-start.1 = ((bf16[8,1,128,512]{2,3,1,0:T(8,128)(2,1)}), bf16[8,1,128,512]{2,3,1,0:T(8,128)(2,1)S(1)}, u32[]{:S(2)}, u32[]{:S(2)}) async-start(bf16[8,1,128,512]{2,3,1,0:T(8,128)(2,1)} %fusion.24), calls=%async_computation.1 | async-start | bytes 2097152 | tf_op jit(solution)/shard_map/all_to_all | solution.py:131
  262.3 3.0 %copy-start.4 = (bf16[512,512]{1,0:T(8,128)(2,1)S(1)}, bf16[512,512]{1,0:T(8,128)(2,1)}, u32[]{:S(2)}) copy-start(bf16[512,512]{1,0:T(8,128)(2,1)} %param.35) | copy-start | bytes 1572868
Sparse Core Ops, SparseCore 0:
  31.0 36.1 all-reduce.2
  102.0 33.3 all-gather.1
